TPU v7x, 512 devices: a whole 4x4x16 slice. The times are simulated.
512 devices in a mesh: dp: 4 (over x), kv: 64 (over z, y), tp: 2 (over core).
Axes of the slice: x: 4, y: 4, z: 16, core: 2. Of those that a mesh axis runs over, the one named last changes fastest.
Arguments:
- tokens: bfloat16 [768, 2048], P('dp', ('kv', 'tp')), may hold values from -21 to 21
- state: float32 [768, 8, 128, 128], P(('dp', 'kv'), 'tp'), may hold values from -3 to 3
- mix_gain: bfloat16 [2048], P(('kv', 'tp')), may hold values from 0.099609375 to 1.8984375
- w_query: bfloat16 [2048, 1024], P('kv', 'tp'), may hold values from -0.125 to 0.125
- w_key: bfloat16 [2048, 1024], P('kv', 'tp'), may hold values from -0.125 to 0.125
- w_value: bfloat16 [2048, 1024], P('kv', 'tp'), may hold values from -0.125 to 0.125
- w_beta: bfloat16 [2048, 8], P('kv', 'tp'), may hold values from -0.125 to 0.125
- w_decay: bfloat16 [2048, 8], P('kv', 'tp'), may hold values from -0.125 to 0.125
- decay_log: float32 [8], P('tp'), may hold values from -1.5 to 1
- head_gain: bfloat16 [128], replicated, may hold values from 0.099609375 to 1.8984375
- w_out: bfloat16 [1024, 2048], P('tp', 'kv'), may hold values from -0.1875 to 0.1875
- ff_gain: bfloat16 [2048], P(('kv', 'tp')), may hold values from 0.099609375 to 1.8984375
- w_up: bfloat16 [2048, 8192], P(None, ('kv', 'tp')), may hold values from -0.125 to 0.125
- w_down: bfloat16 [8192, 2048], P(('kv', 'tp')), may hold values from -0.25 to 0.25
Outputs:
- output: bfloat16 [768, 2048], P('dp', ('kv', 'tp'))
- new_state: float32 [768, 8, 128, 128], P(('dp', 'kv'), 'tp')
All inputs are finite; a program needn't handle non-finite values.
Results may differ from a plain program's by a relative error of at most 0.013.
Values may be sent and summed in bfloat16 or wider, within the bound.
A program may use at most 64 MiB of HBM per device.

v0:
```python
import math
import jax
import jax.numpy as jnp
from jax import lax
from jax.sharding import PartitionSpec as P

D = 2048


def gather_turned(arrays, axis, dims):
    turned = [jnp.moveaxis(a, dim, 0) for a, dim in zip(arrays, dims)]
    both = jnp.concatenate([t.reshape(len(t), -1) for t in turned], axis=1)
    filled, at, finished = (lax.all_gather(both, axis, axis=0, tiled=True), 0, [])
    for t, dim in zip(turned, dims):
        slab = filled[:, at : at + t[0].size].reshape(-1, *t.shape[1:])
        finished.append(jnp.moveaxis(slab, 0, dim))
        at += t[0].size
    return tuple(finished)


def in_blocks(value, dim, size):
    before, after = (value.shape[:dim], value.shape[dim + 1 :])
    return jnp.moveaxis(value.reshape(*before, size, -1, *after), dim, 0)


def sent_and_summed(value, axis, dim):
    size = lax.axis_size(axis)
    pieces = lax.all_to_all(in_blocks(value, dim, size), axis, 0, 0, tiled=True)
    return jnp.sum(pieces.astype(jnp.float32), axis=0)


def in_one_piece(arrays, axis, dim, along):
    widths = [math.prod(a.shape[along:]) for a in arrays]
    both = jnp.concatenate(
        [a.reshape(*a.shape[:along], w) for a, w in zip(arrays, widths)], axis=along
    )
    filled = sent_and_summed(both, axis, dim)
    pieces = jnp.split(filled, [sum(widths[:k]) for k in range(1, len(widths))], axis=along)
    return tuple(
        (b.reshape(*filled.shape[:along], *a.shape[along:]) for a, b in zip(arrays, pieces))
    )


def copy_for_each(value, axis):
    copies = jnp.broadcast_to(value, (lax.axis_size(axis), *value.shape))
    return lax.all_to_all(copies, axis, split_axis=0, concat_axis=0, tiled=True)


def in_order(pieces, dim):
    pieces = jnp.moveaxis(pieces, 0, dim)
    shape = pieces.shape
    return pieces.reshape(*shape[:dim], shape[dim] * shape[dim + 1], *shape[dim + 2 :])


def collect(value, axis, dim):
    pieces = copy_for_each(value, axis)
    return in_order(pieces, dim)


def one_gather(arrays, axis, dims):
    vector = jnp.concatenate([a.reshape(-1) for a in arrays])
    lines, at, finished = (lax.all_gather(vector, axis), 0, [])
    for a, dim in zip(arrays, dims):
        pieces = lines[:, at : at + a.size].reshape(-1, *a.shape)
        finished.append(in_order(pieces, dim))
        at += a.size
    return tuple(finished)


def local(
    tokens,
    state,
    mix_gain,
    w_query,
    w_key,
    w_value,
    w_beta,
    w_decay,
    decay_log,
    head_gain,
    w_out,
    ff_gain,
    w_up,
    w_down,
):
    seq_count = state.shape[0]
    heads_local = state.shape[1]
    head_size = state.shape[2]
    tokens_wide, gain_wide = gather_turned((tokens, mix_gain[None, :]), "tp", (1, 1))
    wide_float = tokens_wide.astype(jnp.float32)
    scaled = (wide_float * gain_wide.astype(jnp.float32)).astype(jnp.bfloat16)
    query_part = jnp.dot(scaled, w_query, preferred_element_type=jnp.float32)
    key_part = jnp.dot(scaled, w_key, preferred_element_type=jnp.float32)
    value_part = jnp.dot(scaled, w_value, preferred_element_type=jnp.float32)
    gate_part = jnp.concatenate(
        [
            jnp.dot(scaled, w_beta, preferred_element_type=jnp.float32),
            jnp.dot(scaled, w_decay, preferred_element_type=jnp.float32),
        ],
        axis=1,
    )
    square_part = jnp.sum(wide_float * wide_float, axis=1)
    query_sum, key_sum, value_sum, gate_sum, square_sum = in_one_piece(
        (
            query_part.astype(jnp.bfloat16),
            key_part.astype(jnp.bfloat16),
            value_part.astype(jnp.bfloat16),
            gate_part.astype(jnp.bfloat16),
            square_part.astype(jnp.bfloat16),
        ),
        "kv",
        0,
        1,
    )
    inverse = lax.rsqrt(square_sum / D + 1e-06)[:, None]
    query = (inverse * query_sum).reshape(seq_count, heads_local, head_size)
    key_rows = (inverse * key_sum).reshape(seq_count, heads_local, head_size)
    value = (inverse * value_sum).reshape(seq_count, heads_local, head_size)
    gates = inverse * gate_sum
    beta = jax.nn.sigmoid(gates[:, :heads_local])
    decay = -jnp.exp(decay_log)[None, :] * jax.nn.softplus(gates[:, heads_local:])
    qnorm = query * lax.rsqrt(jnp.sum(query * query, axis=-1, keepdims=True) + 1e-06)
    knorm = key_rows * lax.rsqrt(jnp.sum(key_rows * key_rows, axis=-1, keepdims=True) + 1e-06)
    kept = state * jnp.exp(decay)[:, :, None, None]
    predicted = jnp.sum(kept * knorm[:, :, :, None], axis=2)
    new_state = (
        kept + (beta[:, :, None] * knorm)[:, :, :, None] * (value - predicted)[:, :, None, :]
    )
    heads = jnp.sum(new_state * qnorm[:, :, :, None], axis=2) / jnp.sqrt(jnp.float32(head_size))
    normed = (
        heads
        * lax.rsqrt(jnp.mean(heads * heads, axis=-1, keepdims=True) + 1e-06)
        * head_gain.astype(jnp.float32)
    )
    normed = normed.astype(jnp.bfloat16).reshape(seq_count, heads_local * head_size)
    partial_mix = jnp.dot(collect(normed, "kv", 0), w_out, preferred_element_type=jnp.float32)
    mixed = sent_and_summed(partial_mix.astype(jnp.bfloat16), "tp", 1)
    resid = (tokens.astype(jnp.float32) + mixed).astype(jnp.bfloat16)
    up_weight, down_weight, gain_pair = one_gather(
        (w_up, w_down, ff_gain[None, :]), "tp", (1, 0, 1)
    )
    gain_local = gain_pair[0]
    work_rows = lax.all_to_all(resid, "tp", split_axis=0, concat_axis=1, tiled=True)
    resid_float = work_rows.astype(jnp.float32)
    whole_rows, whole_gain = gather_turned((work_rows, gain_local[None, :]), "kv", (1, 1))
    whole_float = whole_rows.astype(jnp.float32)
    inverse2 = lax.rsqrt(jnp.mean(whole_float * whole_float, axis=1, keepdims=True) + 1e-06)
    scaled2 = (whole_float * whole_gain.astype(jnp.float32)).astype(jnp.bfloat16)
    up_rows = jnp.dot(scaled2, up_weight, preferred_element_type=jnp.float32) * inverse2
    act = jnp.square(jax.nn.relu(up_rows)).astype(jnp.bfloat16)
    summed = sent_and_summed(
        lax.dot_general(
            down_weight, act, (((0,), (1,)), ((), ())), preferred_element_type=jnp.float32
        ).astype(jnp.bfloat16),
        "kv",
        0,
    )
    results = (resid_float + summed.T).astype(jnp.bfloat16)
    output = results
    output = lax.all_to_all(output, "tp", split_axis=1, concat_axis=0, tiled=True)
    return (output, new_state)


def solution(mesh):
    placed = (
        P("dp", ("kv", "tp")),
        P(("dp", "kv"), "tp", None, None),
        P(("kv", "tp")),
        P("kv", "tp"),
        P("kv", "tp"),
        P("kv", "tp"),
        P("kv", "tp"),
        P("kv", "tp"),
        P("tp"),
        P(),
        P("tp", "kv"),
        P(("kv", "tp")),
        P(None, ("kv", "tp")),
        P(("kv", "tp"), None),
    )
    return jax.shard_map(
        local,
        mesh=mesh,
        in_specs=placed,
        out_specs=(P("dp", ("kv", "tp")), P(("dp", "kv"), "tp", None, None)),
        check_vma=False,
    )
```

profile of v0, /device:TPU:1, one launch (start us, length us, event | category | flops | bytes accessed | tf_op | source)
XLA Modules:
  0.0 285.4 jit_solution(2601442207486391683)
XLA Ops:
  7.2 0.8 copy.104
  7.9 0.8 pad_maximum_fusion.1
  8.7 8.3 %all_gather.12 = bf16[32,193]{1,0:T(8,128)(2,1)S(1)} all-gather(bf16[16,193]{1,0:T(8,128)(2,1)S(1)} %pad_maximum_fusion.1), channel_id=1, replica_groups=mesh['dp'=4,'kv'=64,'tp'=2] {'tp'}, dimensions={0}, use_global_device_ids=true | all-gather | bytes 18528 | tf_op jit(solution)/shard_map/all_gather | solution.py:13
  17.0 0.2 convert_reduce_fusion.4
  17.2 0.3 convolution_convert_fusion.3
  17.7 1.1 convolution_convert_fusion.2
  18.9 0.3 convolution_convert_fusion.1
  19.3 0.2 convolution_convert_fusion.6
  19.5 0.2 concatenate.31
  19.7 0.5 copy.105
  20.2 0.2 convolution_convert_fusion.5
  20.4 0.2 concatenate.32
  20.6 0.5 copy.106
  21.1 0.2 convert_element_type.127
  21.3 2.0 concatenate.33
  23.3 13.2 %all-to-all-start = ((bf16[64,3,1545]{2,1,0:T(4,128)(2,1)}), bf16[64,3,1545]{2,1,0:T(4,128)(2,1)S(1)}, u32[]{:S(2)}, u32[]{:S(2)}) async-start(bf16[64,3,1545]{2,1,0:T(4,128)(2,1)} %concatenate.33), calls=%async_computation | async-start | bytes 1703936 | tf_op jit(solution)/shard_map/all_to_all | solution.py:28
  36.7 0.3 copy.115
  37.0 0.3 reshape.146
  37.3 1.3 dynamic-slice
  39.3 4.9 %dynamic-update-slice = bf16[524320]{0:T(1024)(128)(2,1)S(1)} dynamic-update-slice(bf16[524320]{0:T(1024)(128)(2,1)S(1)} %broadcast.84, bf16[262160]{0:T(1024)(128)(2,1)S(1)} %pad_maximum_fusion, u32[]{:T(128)} %bitcast.7) | dynamic-update-slice | bytes 1048644
  44.2 1.0 copy-done.1
  45.2 43.0 %all-reduce.3.cloned.1.call-done = bf16[524320]{0:T(1024)(128)(2,1)} async-done(((bf16[524320]{0:T(1024)(128)(2,1)}), bf16[524320]{0:T(1024)(128)(2,1)}) %all-reduce.3.cloned.1.call-update) | async-done | bytes 1048656
  88.2 2.6 reshape.153
  90.9 0.4 convert_reduce_fusion
  91.2 0.2 fusion.21
  92.4 0.3 multiply_reduce_fusion.1
  92.7 1.4 multiply_reduce_fusion
  94.5 0.8 broadcast_in_dim.2
  95.2 14.4 %all-to-all-start.1 = ((bf16[64,3,512]{2,1,0:T(4,128)(2,1)}), bf16[64,3,512]{2,1,0:T(4,128)(2,1)S(1)}, u32[]{:S(2)}, u32[]{:S(2)}) async-start(bf16[64,3,512]{2,1,0:T(4,128)(2,1)} %broadcast_in_dim.2), calls=%async_computation.1 | async-start | bytes 524288 | tf_op jit(solution)/shard_map/all_to_all | solution.py:46
  109.6 0.7 fusion.28
  110.3 0.5 reshape_reshape.3
  110.8 0.7 reshape.148
  111.5 0.3 copy.117
  111.9 0.3 slice-done
  112.2 17.7 %all-to-all-done.1 = bf16[64,3,512]{2,1,0:T(4,128)(2,1)S(1)} async-done(((bf16[64,3,512]{2,1,0:T(4,128)(2,1)}), bf16[64,3,512]{2,1,0:T(4,128)(2,1)S(1)}, u32[]{:S(2)}, u32[]{:S(2)}) %all-to-all-start.1) | async-done | bytes 196640 | tf_op jit(solution)/shard_map/all_to_all | solution.py:46
  130.0 0.2 reshape.144
  130.2 0.1 convolution_convert_fusion.4
  130.3 6.5 %all_to_all.58 = bf16[2,192,16]{1,2,0:T(8,128)(2,1)S(1)} all-to-all(bf16[2,192,16]{1,2,0:T(8,128)(2,1)S(1)} %bitcast.54), channel_id=1, replica_groups=mesh['dp'=4,'kv'=64,'tp'=2] {'tp'}, dimensions={0} | all-to-all | bytes 24576 | tf_op jit(solution)/shard_map/all_to_all | solution.py:28
  136.9 3.7 %all_to_all.59 = bf16[2,96,16]{1,2,0:T(8,128)(2,1)S(1)} all-to-all(bf16[2,96,16]{1,2,0:T(8,128)(2,1)S(1)} %copy.114), channel_id=1, replica_groups=mesh['dp'=4,'kv'=64,'tp'=2] {'tp'}, dimensions={0} | all-to-all | bytes 12288 | tf_op jit(solution)/shard_map/all_to_all | solution.py:143
  140.7 72.8 %all_gather.15 = bf16[2048,97]{1,0:T(8,128)(2,1)S(1)} all-gather(bf16[32,97]{1,0:T(8,128)(2,1)S(1)} %pad_maximum_fusion.2), channel_id=1, replica_groups=mesh['dp'=4,'kv'=64,'tp'=2] {'kv'}, dimensions={0}, use_global_device_ids=true | all-gather | bytes 403520 | tf_op jit(solution)/shard_map/all_gather | solution.py:13
  213.5 0.4 convert_reduce_fusion.1
  213.9 0.3 fusion.4
  214.2 1.1 convolution_convert_fusion
  215.3 0.3 copy.118
  215.6 27.9 %all_to_all.60 = bf16[64,32,96]{2,1,0:T(8,128)(2,1)S(1)} all-to-all(bf16[64,32,96]{2,1,0:T(8,128)(2,1)S(1)} %bitcast.50), channel_id=1, replica_groups=mesh['dp'=4,'kv'=64,'tp'=2] {'kv'}, dimensions={0} | all-to-all | bytes 786432 | tf_op jit(solution)/shard_map/all_to_all | solution.py:28
  243.4 0.1 convert_reduce_fusion.2
  243.6 34.2 %all_to_all.61 = bf16[96,2,16]{0,2,1:T(8,128)(2,1)S(1)} all-to-all(bf16[96,2,16]{0,2,1:T(8,128)(2,1)S(1)} %bitcast.57), channel_id=1, replica_groups=mesh['dp'=4,'kv'=64,'tp'=2] {'tp'}, dimensions={1} | all-to-all | bytes 12288 | tf_op jit(solution)/shard_map/all_to_all | solution.py:160
  277.8 0.7 all_to_all.51
  (72 shorter events, 2.3 us)
Async XLA Ops:
  7.2 10.1 %copy-start = (bf16[32,512]{1,0:T(8,128)(2,1)S(1)}, bf16[32,512]{1,0:T(8,128)(2,1)}, u32[]{:S(2)}) copy-start(bf16[32,512]{1,0:T(8,128)(2,1)} %param.17) | copy-start | bytes 98308
  7.2 11.7 %copy-start.6 = (bf16[32,512]{1,0:T(8,128)(2,1)S(1)}, bf16[32,512]{1,0:T(8,128)(2,1)}, u32[]{:S(2)}) copy-start(bf16[32,512]{1,0:T(8,128)(2,1)} %param.19) | copy-start | bytes 98308
  17.2 2.1 copy-start.10
  17.5 2.6 copy-start.11
  23.3 13.3 %copy-start.5 = (bf16[64,2048]{1,0:T(8,128)(2,1)S(1)}, bf16[64,2048]{1,0:T(8,128)(2,1)}, u32[]{:S(2)}) copy-start(bf16[64,2048]{1,0:T(8,128)(2,1)} %param.27) | copy-start | bytes 786436
  23.3 13.4 %copy-start.4 = (bf16[2048,64]{0,1:T(8,128)(2,1)S(1)}, bf16[2048,64]{0,1:T(8,128)(2,1)}, u32[]{:S(2)}) copy-start(bf16[2048,64]{0,1:T(8,128)(2,1)} %param.26) | copy-start | bytes 786436
  23.3 67.6 %all-to-all-start = ((bf16[64,3,1545]{2,1,0:T(4,128)(2,1)}), bf16[64,3,1545]{2,1,0:T(4,128)(2,1)S(1)}, u32[]{:S(2)}, u32[]{:S(2)}) async-start(bf16[64,3,1545]{2,1,0:T(4,128)(2,1)} %concatenate.33), calls=%async_computation | async-start | bytes 1703936 | tf_op jit(solution)/shard_map/all_to_all | solution.py:28
  36.5 0.7 copy-start.9
  36.6 51.7 %all-reduce.3.cloned.1.call-start = ((), (), s32[]{:S(2)}) async-start(), calls=%async_computation.6 | async-start | bytes 2101248
  39.3 5.9 %copy-start.12 = (bf16[128]{0:T(256)(128)(2,1)S(1)}, bf16[128]{0:T(256)(128)(2,1)}, u32[]{:S(2)}) copy-start(bf16[128]{0:T(256)(128)(2,1)} %param.23) | copy-start | bytes 772
  39.3 5.9 %copy-start.13 = (f32[4]{0:T(128)S(1)}, f32[4]{0:T(128)}, u32[]{:S(2)}) copy-start(f32[4]{0:T(128)} %param.22) | copy-start | bytes 52
  44.2 1.0 copy-start.1
  90.8 19.5 %copy-start.2 = (bf16[2,262160]{1,0:T(2,128)(2,1)}, bf16[2,262160]{1,0:T(2,128)(2,1)S(1)}, u32[]{:S(2)}) copy-start(bf16[2,262160]{1,0:T(2,128)(2,1)S(1)} %reshape.153) | copy-start | bytes 3145924
  90.8 1.6 copy-start.3
  95.2 34.7 %all-to-all-start.1 = ((bf16[64,3,512]{2,1,0:T(4,128)(2,1)}), bf16[64,3,512]{2,1,0:T(4,128)(2,1)S(1)}, u32[]{:S(2)}, u32[]{:S(2)}) async-start(bf16[64,3,512]{2,1,0:T(4,128)(2,1)} %broadcast_in_dim.2), calls=%async_computation.1 | async-start | bytes 524288 | tf_op jit(solution)/shard_map/all_to_all | solution.py:46
  111.5 0.7 slice-start
  111.5 18.7 %copy-start.7 = (bf16[512,32]{0,1:T(8,128)(2,1)S(1)}, bf16[512,32]{0,1:T(8,128)(2,1)}, u32[]{:S(2)}) copy-start(bf16[512,32]{0,1:T(8,128)(2,1)} %param.24) | copy-start | bytes 98308
  111.5 25.3 %copy-start.8 = (bf16[192,16]{0,1:T(8,128)(2,1)S(1)}, bf16[192,16]{0,1:T(8,128)(2,1)}, u32[]{:S(2)}) copy-start(bf16[192,16]{0,1:T(8,128)(2,1)} %param.14) | copy-start | bytes 18436
Sparse Core Ops, SparseCore 0:
  45.3 42.8 all-reduce.2
where the time goes:
time: 286 us; the launch traced here: 285 us
  blocking collectives  153 us (53%)
  waiting for transfers between devices  60.7 us (21%)
  starting transfers between devices  27.6 us (10%)
  local copies, waits for them, and re-layouts  20.3 us (7%)
  between operations  15.1 us (5%)
  other arithmetic  4.86 us (2%)
  matrix products  3.28 us (1%)
    all_gather x2, blocking collectives, gather_turned(): lax.all_gather(both, axis, axis=0, tiled=True)  81.1 us
    unnamed x2, waiting for transfers between devices  43 us
    all_to_all x2, blocking collectives, sent_and_summed(): pieces = lax.all_to_all(in_blocks(value, dim, size), axis, 0, 0, tiled=True)  34.3 us
    all_to_all x1, blocking collectives, local(): lax.all_to_all(output, 'tp', split_axis=1, concat_axis=0, tiled=True)  34.2 us
    all_to_all x1, waiting for transfers between devices, copy_for_each(): return lax.all_to_all(copies, axis, split_axis=0, concat_axis=0, tiled=True)  17.7 us
    all_to_all x1, starting transfers between devices, copy_for_each(): return lax.all_to_all(copies, axis, split_axis=0, concat_axis=0, tiled=True)  14.4 us
    all_to_all x1, starting transfers between devices, sent_and_summed(): pieces = lax.all_to_all(in_blocks(value, dim, size), axis, 0, 0, tiled=True)  13.2 us
    unnamed x35, local copies, waits for them, and re-layouts  7.79 us
  transfers between devices with their start and end apart: 3, of which 2 were waited for; matrix products, arithmetic and copies ran while one was open for 4% of the time, Pallas kernels for 0%

commit v1 on v0

--- a/solution.py
+++ b/solution.py
@@ -10,7 +10,13 @@
 def gather_turned(arrays, axis, dims):
     turned = [jnp.moveaxis(a, dim, 0) for a, dim in zip(arrays, dims)]
     both = jnp.concatenate([t.reshape(len(t), -1) for t in turned], axis=1)
-    filled, at, finished = (lax.all_gather(both, axis, axis=0, tiled=True), 0, [])
+    filled, at, finished = (
+        jnp.concatenate(
+            lax.all_to_all(jnp.stack([both] * lax.axis_size(axis)), axis, 0, 0), axis=0
+        ),
+        0,
+        [],
+    )
     for t, dim in zip(turned, dims):
         slab = filled[:, at : at + t[0].size].reshape(-1, *t.shape[1:])
         finished.append(jnp.moveaxis(slab, 0, dim))

time: 286 us -> 218 us (0.76)
  blocking collectives: 153 us -> 65.8 us
  waiting for transfers between devices: 60.7 us -> 80.1 us
    all_gather x2 -> x0, blocking collectives: 81.1 us -> none  [gather_turned(): lax.all_gather(both, axis, axis=0, tiled=True)]
    unnamed x2, waiting for transfers between devices: 43 us -> 0.04 us
    all_to_all x1, waiting for transfers between devices: 0.01 us -> 34.9 us  [sent_and_summed(): pieces = lax.all_to_all(in_blocks(value, dim, size), axis, 0, 0, tiled=True)]
    all_to_all x0 -> x1, waiting for transfers between devices: none -> 28.8 us  [gather_turned(): lax.all_to_all(jnp.stack([both] * lax.axis_size(axis)), axis, 0, 0)]
    all_to_all x1, blocking collectives: 34.2 us -> 7.75 us  [local(): lax.all_to_all(output, 'tp', split_axis=1, concat_axis=0, tiled=True)]
    all_to_all x0 -> x1, blocking collectives: none -> 10.2 us  [gather_turned(): lax.all_to_all(jnp.stack([both] * lax.axis_size(axis)), axis, 0, 0)]
    all_to_all x2, blocking collectives: 34.3 us -> 44.1 us  [sent_and_summed(): pieces = lax.all_to_all(in_blocks(value, dim, size), axis, 0, 0, tiled=True)]
    all_to_all x1, starting transfers between devices: 14.4 us -> 8.59 us  [copy_for_each(): return lax.all_to_all(copies, axis, split_axis=0, concat_axis=0, tiled=True)]
  transfers between devices with their start and end apart: 3 -> 4, of which waited for: 2 -> 3; matrix products, arithmetic and copies ran while one was open for 4% -> 7% of each run, Pallas kernels for 0% -> 0%
where the time goes in v1:
time: 218 us; the launch traced here: 217 us
  waiting for transfers between devices  80.1 us (37%)
  blocking collectives  65.8 us (30%)
  starting transfers between devices  26.7 us (12%)
  local copies, waits for them, and re-layouts  21.2 us (10%)
  between operations  15.1 us (7%)
  other arithmetic  4.69 us (2%)
  matrix products  3.28 us (2%)
    all_to_all x2, blocking collectives, sent_and_summed(): pieces = lax.all_to_all(in_blocks(value, dim, size), axis, 0, 0, tiled=True)  44.1 us
    all_to_all x1, waiting for transfers between devices, sent_and_summed(): pieces = lax.all_to_all(in_blocks(value, dim, size), axis, 0, 0, tiled=True)  34.9 us
    all_to_all x1, waiting for transfers between devices, gather_turned(): lax.all_to_all(jnp.stack([both] * lax.axis_size(axis)), axis, 0, 0)  28.8 us
    all_to_all x1, waiting for transfers between devices, copy_for_each(): return lax.all_to_all(copies, axis, split_axis=0, concat_axis=0, tiled=True)  16.4 us
    all_to_all x1, starting transfers between devices, sent_and_summed(): pieces = lax.all_to_all(in_blocks(value, dim, size), axis, 0, 0, tiled=True)  13.2 us
    all_to_all x1, blocking collectives, gather_turned(): lax.all_to_all(jnp.stack([both] * lax.axis_size(axis)), axis, 0, 0)  10.2 us
    all_to_all x1, starting transfers between devices, copy_for_each(): return lax.all_to_all(copies, axis, split_axis=0, concat_axis=0, tiled=True)  8.59 us
    unnamed x34, local copies, waits for them, and re-layouts  7.9 us
  transfers between devices with their start and end apart: 4, of which 3 were waited for; matrix products, arithmetic and copies ran while one was open for 7% of the time, Pallas kernels for 0%

profile of v1, /device:TPU:1, one launch (start us, length us, event | category | flops | bytes accessed | tf_op | source)
XLA Modules:
  0.0 216.9 jit_solution(10695446534793306176)
XLA Ops:
  7.2 0.8 copy.112
  7.9 0.8 maximum_bitcast_fusion
  8.7 10.2 %all_to_all.68 = bf16[2,16,193]{2,1,0:T(8,128)(2,1)S(1)} all-to-all(bf16[2,16,193]{2,1,0:T(8,128)(2,1)S(1)} %pad_maximum_fusion.1), channel_id=1, replica_groups=mesh['dp'=4,'kv'=64,'tp'=2] {'tp'}, dimensions={0} | all-to-all | bytes 24704 | tf_op jit(solution)/shard_map/all_to_all | solution.py:15
  19.2 0.3 convolution_convert_fusion.3
  19.6 1.1 convolution_convert_fusion.2
  20.8 0.3 convolution_convert_fusion.1
  21.2 0.2 convolution_convert_fusion.6
  21.4 0.2 concatenate.31
  21.6 0.5 copy.114
  22.1 0.2 convolution_convert_fusion.5
  22.3 0.2 concatenate.32
  22.5 0.5 copy.115
  23.0 0.2 convert_element_type.127
  23.2 2.0 concatenate.33
  25.2 13.2 %all-to-all-start.1 = ((bf16[64,3,1545]{2,1,0:T(4,128)(2,1)}), bf16[64,3,1545]{2,1,0:T(4,128)(2,1)S(1)}, u32[]{:S(2)}, u32[]{:S(2)}) async-start(bf16[64,3,1545]{2,1,0:T(4,128)(2,1)} %concatenate.33), calls=%async_computation.1 | async-start | bytes 1703936 | tf_op jit(solution)/shard_map/all_to_all | solution.py:34
  38.6 0.3 copy.124
  38.9 0.3 reshape.155
  39.2 1.3 dynamic-slice
  41.2 4.9 %dynamic-update-slice = bf16[524320]{0:T(1024)(128)(2,1)S(1)} dynamic-update-slice(bf16[524320]{0:T(1024)(128)(2,1)S(1)} %broadcast.86, bf16[262160]{0:T(1024)(128)(2,1)S(1)} %pad_maximum_fusion, u32[]{:T(128)} %bitcast.10) | dynamic-update-slice | bytes 1048644
  46.2 1.0 copy-done.1
  47.2 34.9 %all-to-all-done.1 = bf16[64,3,1545]{2,1,0:T(4,128)(2,1)S(1)} async-done(((bf16[64,3,1545]{2,1,0:T(4,128)(2,1)}), bf16[64,3,1545]{2,1,0:T(4,128)(2,1)S(1)}, u32[]{:S(2)}, u32[]{:S(2)}) %all-to-all-start.1) | async-done | bytes 593312 | tf_op jit(solution)/shard_map/all_to_all | solution.py:34
  82.2 0.4 convert_reduce_fusion
  82.5 0.2 fusion.21
  83.7 0.3 multiply_reduce_fusion.1
  84.0 1.4 multiply_reduce_fusion
  85.8 0.8 broadcast_in_dim.2
  86.6 8.6 %all-to-all-start.2 = ((bf16[64,3,512]{2,1,0:T(4,128)(2,1)}), bf16[64,3,512]{2,1,0:T(4,128)(2,1)S(1)}, u32[]{:S(2)}, u32[]{:S(2)}) async-start(bf16[64,3,512]{2,1,0:T(4,128)(2,1)} %broadcast_in_dim.2), calls=%async_computation.2 | async-start | bytes 524288 | tf_op jit(solution)/shard_map/all_to_all | solution.py:52
  95.2 2.6 %reshape.163 = bf16[2,262160]{1,0:T(2,128)(2,1)S(1)} reshape(bf16[524320]{0:T(1024)(128)(2,1)} %all-reduce.3.cloned.1.call-done) | data formatting | bytes 2097280 | tf_op jit(solution)/shard_map/all_gather | solution.py:68
  97.9 16.4 %all-to-all-done.2 = bf16[64,3,512]{2,1,0:T(4,128)(2,1)S(1)} async-done(((bf16[64,3,512]{2,1,0:T(4,128)(2,1)}), bf16[64,3,512]{2,1,0:T(4,128)(2,1)S(1)}, u32[]{:S(2)}, u32[]{:S(2)}) %all-to-all-start.2) | async-done | bytes 196640 | tf_op jit(solution)/shard_map/all_to_all | solution.py:52
  114.3 0.2 reshape.153
  114.5 0.1 convolution_convert_fusion.4
  114.7 7.9 %all_to_all.69 = bf16[2,192,16]{1,2,0:T(8,128)(2,1)S(1)} all-to-all(bf16[2,192,16]{1,2,0:T(8,128)(2,1)S(1)} %bitcast.71), channel_id=1, replica_groups=mesh['dp'=4,'kv'=64,'tp'=2] {'tp'}, dimensions={0} | all-to-all | bytes 24576 | tf_op jit(solution)/shard_map/all_to_all | solution.py:34
  122.6 3.7 %all_to_all.70 = bf16[2,96,16]{1,2,0:T(8,128)(2,1)S(1)} all-to-all(bf16[2,96,16]{1,2,0:T(8,128)(2,1)S(1)} %copy.123), channel_id=1, replica_groups=mesh['dp'=4,'kv'=64,'tp'=2] {'tp'}, dimensions={0} | all-to-all | bytes 12288 | tf_op jit(solution)/shard_map/all_to_all | solution.py:149
  126.4 0.9 stack.8
  127.3 4.8 %all-to-all-start.5 = ((bf16[64,32,97]{2,1,0:T(8,128)(2,1)}), bf16[64,32,97]{2,1,0:T(8,128)(2,1)S(1)}, u32[]{:S(2)}, u32[]{:S(2)}) async-start(bf16[64,32,97]{2,1,0:T(8,128)(2,1)} %stack.8), calls=%async_computation.5 | async-start | bytes 1048576 | tf_op jit(solution)/shard_map/all_to_all | solution.py:15
  132.1 0.7 fusion.28
  132.8 0.5 reshape_reshape.3
  133.3 0.7 reshape.158
  134.0 0.4 copy.126
  134.3 28.8 %all-to-all-done.5 = bf16[64,32,97]{2,1,0:T(8,128)(2,1)S(1)} async-done(((bf16[64,32,97]{2,1,0:T(8,128)(2,1)}), bf16[64,32,97]{2,1,0:T(8,128)(2,1)S(1)}, u32[]{:S(2)}, u32[]{:S(2)}) %all-to-all-start.5) | async-done | bytes 397344 | tf_op jit(solution)/shard_map/all_to_all | solution.py:15
  163.1 0.4 convert_reduce_fusion.1
  163.5 0.3 fusion.4
  163.8 1.1 convolution_convert_fusion
  164.9 0.3 copy.127
  165.2 36.3 %all_to_all.71 = bf16[64,32,96]{2,1,0:T(8,128)(2,1)S(1)} all-to-all(bf16[64,32,96]{2,1,0:T(8,128)(2,1)S(1)} %bitcast.60), channel_id=1, replica_groups=mesh['dp'=4,'kv'=64,'tp'=2] {'kv'}, dimensions={0} | all-to-all | bytes 786432 | tf_op jit(solution)/shard_map/all_to_all | solution.py:34
  201.4 0.1 convert_reduce_fusion.2
  201.6 7.7 %all_to_all.72 = bf16[96,2,16]{0,2,1:T(8,128)(2,1)S(1)} all-to-all(bf16[96,2,16]{0,2,1:T(8,128)(2,1)S(1)} %bitcast.74), channel_id=1, replica_groups=mesh['dp'=4,'kv'=64,'tp'=2] {'tp'}, dimensions={1} | all-to-all | bytes 12288 | tf_op jit(solution)/shard_map/all_to_all | solution.py:166
  209.3 0.7 all_to_all.59
  (74 shorter events, 2.5 us)
Async XLA Ops:
  7.2 12.0 %copy-start = (bf16[32,512]{1,0:T(8,128)(2,1)S(1)}, bf16[32,512]{1,0:T(8,128)(2,1)}, u32[]{:S(2)}) copy-start(bf16[32,512]{1,0:T(8,128)(2,1)} %param.17) | copy-start | bytes 98308
  7.2 13.6 %copy-start.5 = (bf16[32,512]{1,0:T(8,128)(2,1)S(1)}, bf16[32,512]{1,0:T(8,128)(2,1)}, u32[]{:S(2)}) copy-start(bf16[32,512]{1,0:T(8,128)(2,1)} %param.19) | copy-start | bytes 98308
  19.1 2.1 copy-start.9
  19.5 2.6 %copy-start.10 = (bf16[32,4]{0,1:T(4,128)(2,1)S(1)}, bf16[32,4]{0,1:T(4,128)(2,1)}, u32[]{:S(2)}) copy-start(bf16[32,4]{0,1:T(4,128)(2,1)} %param.21) | copy-start | bytes 772
  25.2 13.3 %copy-start.4 = (bf16[64,2048]{1,0:T(8,128)(2,1)S(1)}, bf16[64,2048]{1,0:T(8,128)(2,1)}, u32[]{:S(2)}) copy-start(bf16[64,2048]{1,0:T(8,128)(2,1)} %param.27) | copy-start | bytes 786436
  25.2 13.4 %copy-start.3 = (bf16[2048,64]{0,1:T(8,128)(2,1)S(1)}, bf16[2048,64]{0,1:T(8,128)(2,1)}, u32[]{:S(2)}) copy-start(bf16[2048,64]{0,1:T(8,128)(2,1)} %param.26) | copy-start | bytes 786436
  25.2 56.9 %all-to-all-start.1 = ((bf16[64,3,1545]{2,1,0:T(4,128)(2,1)}), bf16[64,3,1545]{2,1,0:T(4,128)(2,1)S(1)}, u32[]{:S(2)}, u32[]{:S(2)}) async-start(bf16[64,3,1545]{2,1,0:T(4,128)(2,1)} %concatenate.33), calls=%async_computation.1 | async-start | bytes 1703936 | tf_op jit(solution)/shard_map/all_to_all | solution.py:34
  38.5 56.7 %all-reduce.3.cloned.1.call-start = ((), (), s32[]{:S(2)}) async-start(), calls=%async_computation.8 | async-start | bytes 2101248
  38.5 2.5 %copy-start.8 = (bf16[16]{0:T(256)(128)(2,1)S(1)}, bf16[16]{0:T(256)(128)(2,1)}, u32[]{:S(2)}) copy-start(bf16[16]{0:T(256)(128)(2,1)} %param.25) | copy-start | bytes 100
  41.2 6.0 %copy-start.11 = (bf16[128]{0:T(256)(128)(2,1)S(1)}, bf16[128]{0:T(256)(128)(2,1)}, u32[]{:S(2)}) copy-start(bf16[128]{0:T(256)(128)(2,1)} %param.23) | copy-start | bytes 772
  41.2 6.0 %copy-start.12 = (f32[4]{0:T(128)S(1)}, f32[4]{0:T(128)}, u32[]{:S(2)}) copy-start(f32[4]{0:T(128)} %param.22) | copy-start | bytes 52
  46.1 1.0 copy-start.1
  46.1 37.6 %copy-start.2 = (f32[3,4,128,128]{3,2,1,0:T(8,128)S(1)}, f32[3,4,128,128]{3,2,1,0:T(8,128)}, u32[]{:S(2)}) copy-start(f32[3,4,128,128]{3,2,1,0:T(8,128)} %param.15) | copy-start | bytes 2359300
  86.6 27.8 %all-to-all-start.2 = ((bf16[64,3,512]{2,1,0:T(4,128)(2,1)}), bf16[64,3,512]{2,1,0:T(4,128)(2,1)S(1)}, u32[]{:S(2)}, u32[]{:S(2)}) async-start(bf16[64,3,512]{2,1,0:T(4,128)(2,1)} %broadcast_in_dim.2), calls=%async_computation.2 | async-start | bytes 524288 | tf_op jit(solution)/shard_map/all_to_all | solution.py:52
  95.2 19.3 %copy-start.6 = (bf16[512,32]{0,1:T(8,128)(2,1)S(1)}, bf16[512,32]{0,1:T(8,128)(2,1)}, u32[]{:S(2)}) copy-start(bf16[512,32]{0,1:T(8,128)(2,1)} %param.24) | copy-start | bytes 98308
  95.2 27.3 %copy-start.7 = (bf16[192,16]{0,1:T(8,128)(2,1)S(1)}, bf16[192,16]{0,1:T(8,128)(2,1)}, u32[]{:S(2)}) copy-start(bf16[192,16]{0,1:T(8,128)(2,1)} %param.14) | copy-start | bytes 18436
  127.3 35.8 %all-to-all-start.5 = ((bf16[64,32,97]{2,1,0:T(8,128)(2,1)}), bf16[64,32,97]{2,1,0:T(8,128)(2,1)S(1)}, u32[]{:S(2)}, u32[]{:S(2)}) async-start(bf16[64,32,97]{2,1,0:T(8,128)(2,1)} %stack.8), calls=%async_computation.5 | async-start | bytes 1048576 | tf_op jit(solution)/shard_map/all_to_all | solution.py:15
Sparse Core Ops, SparseCore 0:
  47.3 42.8 all-reduce.2
